TPU v7x, 32 devices: a whole 2x2x4 slice. The times are simulated.
32 devices in a mesh: grp: 2 (over y), fs: 4 (over z), tp: 4 (over x, core).
Axes of the slice: x: 2, y: 2, z: 4, core: 2. Of those that a mesh axis runs over, the one named last changes fastest.
Arguments:
- inputs: bfloat16 [6144, 2048], P(('grp', 'fs'), 'tp'), parts along dimension 0, may hold values from -110 to 110, as said below
- mixer_gain: float32 [2048], replicated, may hold values from 0.1 to 1.9
- query_weight: bfloat16 [2048, 1024], P('fs', 'tp'), may hold values from -0.125 to 0.125
- key_weight: bfloat16 [2048, 1024], P('fs', 'tp'), may hold values from -0.125 to 0.125
- value_weight: bfloat16 [2048, 1024], P('fs', 'tp'), may hold values from -0.125 to 0.125
- gate_weight: bfloat16 [2048, 1024], P('fs', 'tp'), may hold values from -0.125 to 0.125
- head_gain: float32 [1024], P('tp'), may hold values from 0.1 to 1.9
- out_weight: bfloat16 [1024, 2048], P('tp', 'fs'), may hold values from -0.1875 to 0.1875
- channel_gain: float32 [2048], replicated, may hold values from 0.1 to 1.9
- up_weight: bfloat16 [2048, 5632], P('fs', 'tp'), may hold values from -0.125 to 0.125
- switch_weight: bfloat16 [2048, 5632], P('fs', 'tp'), may hold values from -0.125 to 0.125
- filter_up: float32 [3, 5632], P(None, 'tp'), may hold values from -3.5 to 3.5
- filter_switch: float32 [3, 5632], P(None, 'tp'), may hold values from -3.5 to 3.5
- down_weight: bfloat16 [5632, 2048], P('tp', 'fs'), may hold values from -0.078125 to 0.078125
Outputs:
- layer_output: bfloat16 [6144, 2048], P(('grp', 'fs'), 'tp'), parts along dimension 0
There are 2 independent parts, one for each index of `grp`. A program takes and returns all parts, laid end to end along the dimension named above; an argument that names none is the same for every part. Nothing has to cross between parts.
Inputs may be any that keep to these rules, and one draw needn't show every extreme that they name: `inputs`: activations of one part.
All inputs are finite; a program needn't handle non-finite values.
Results may differ from a plain program's by a relative error of at most 0.012.
Values may be sent and summed in bfloat16 or wider, within the bound.
A program may use at most 64 MiB of HBM per device.

v0:
```python
import jax
import jax.numpy as jnp
from jax import lax
from jax.sharding import PartitionSpec as P

HEAD = 128


epsilon = 1e-06


def row_norm(row_block, gain_vector):
    values = row_block.astype(jnp.float32)
    scaled = values * lax.rsqrt(jnp.mean(values * values, axis=-1, keepdims=True) + epsilon)
    return (scaled * gain_vector).astype(jnp.bfloat16)


def rotate(field, positions):
    half_width = field.shape[-1] // 2
    frequency = 10000.0 ** (-jnp.arange(half_width, dtype=jnp.float32) * 2.0 / field.shape[-1])
    angles = positions.astype(jnp.float32)[:, None] * frequency[None, :]
    cosine = jnp.cos(angles)[:, None, :]
    sine_part = jnp.sin(angles)[:, None, :]
    first_half = field[..., :half_width]
    second_half = field[..., half_width:]
    return jnp.concatenate(
        [
            first_half * cosine - second_half * sine_part,
            first_half * sine_part + second_half * cosine,
        ],
        axis=-1,
    )


def decays(first_head, count, positions):
    head_ids = (first_head + jnp.arange(count, dtype=jnp.int32)).astype(jnp.float32)
    log_decay = jnp.log1p(-jnp.exp2(-5.0 - head_ids))
    causal = positions[:, None] >= positions[None, :]
    distance = jnp.where(causal, positions[:, None] - positions[None, :], 0).astype(jnp.float32)
    return jnp.where(causal[None], jnp.exp(log_decay[:, None, None] * distance[None]), 0.0)


def retention(query_rows, key_rows, value_rows, gate_rows, gain_vector, first_head):
    length = query_rows.shape[0]
    count = query_rows.shape[1] // HEAD
    positions = jnp.arange(length, dtype=jnp.int32)
    query_rot = rotate(
        query_rows.astype(jnp.float32).reshape(length, count, HEAD), positions
    ).astype(jnp.bfloat16)
    key_rot = rotate(key_rows.astype(jnp.float32).reshape(length, count, HEAD), positions).astype(
        jnp.bfloat16
    )
    decay_table = decays(first_head, count, positions)
    scores = jnp.einsum("thd,shd->hts", query_rot, key_rot, preferred_element_type=jnp.float32)
    weights = (scores * HEAD ** (-0.5) * decay_table).astype(jnp.bfloat16)
    retained = jnp.einsum(
        "hts,shd->thd",
        weights,
        value_rows.reshape(length, count, HEAD),
        preferred_element_type=jnp.float32,
    )
    normalized = retained * lax.rsqrt(
        jnp.mean(retained * retained, axis=-1, keepdims=True) + epsilon
    )
    gated_rows = (
        normalized.reshape(length, count * HEAD)
        * gain_vector
        * jax.nn.silu(gate_rows.astype(jnp.float32))
    )
    return gated_rows.astype(jnp.bfloat16)


def causal_conv(row_block, tap_weights, length):
    sequences = row_block.astype(jnp.float32).reshape(-1, length, row_block.shape[1])
    width_taps = tap_weights.shape[0]
    padded = jnp.pad(sequences, ((0, 0), (width_taps - 1, 0), (0, 0)))
    result = jnp.zeros_like(sequences)
    for tap_index in range(width_taps):
        result = result + padded[:, tap_index : tap_index + length] * tap_weights[tap_index]
    return result.reshape(row_block.shape)


def on_device(
    inputs,
    mixer_gain,
    query_weight,
    key_weight,
    value_weight,
    gate_weight,
    head_gain,
    out_weight,
    channel_gain,
    up_weight,
    switch_weight,
    filter_up,
    filter_switch,
    down_weight,
):
    length = inputs.shape[0]
    rows_whole = lax.all_gather(inputs, "tp", axis=1, tiled=True)
    normed = row_norm(rows_whole, mixer_gain)
    pieces = (
        lax.all_gather(query_weight, "fs", axis=0, tiled=True),
        lax.all_gather(key_weight, "fs", axis=0, tiled=True),
        lax.all_gather(value_weight, "fs", axis=0, tiled=True),
        lax.all_gather(gate_weight, "fs", axis=0, tiled=True),
    )
    columns = normed
    sums = tuple(
        (jnp.dot(columns, matrix, preferred_element_type=jnp.float32) for matrix in pieces)
    )
    query_rows, key_rows, value_rows, gate_rows = [block.astype(jnp.bfloat16) for block in sums]
    local_heads = query_rows.shape[1] // HEAD
    head_out = retention(
        query_rows, key_rows, value_rows, gate_rows, head_gain, lax.axis_index("tp") * local_heads
    )
    partial_value = jnp.dot(
        head_out,
        lax.all_gather(out_weight, "fs", axis=1, tiled=True),
        preferred_element_type=jnp.float32,
    )
    summed = lax.psum_scatter(
        partial_value.astype(jnp.bfloat16), "tp", scatter_dimension=1, tiled=True
    ).astype(jnp.float32)
    mixed_rows = (inputs.astype(jnp.float32) + summed).astype(jnp.bfloat16)
    mixed_whole = lax.all_gather(mixed_rows, "tp", axis=1, tiled=True)
    channel_normed = row_norm(mixed_whole, channel_gain)
    pieces = (
        lax.all_gather(up_weight, "fs", axis=0, tiled=True),
        lax.all_gather(switch_weight, "fs", axis=0, tiled=True),
    )
    columns = channel_normed
    lift_sum = jnp.dot(columns, pieces[0], preferred_element_type=jnp.float32)
    switch_sum = jnp.dot(columns, pieces[1], preferred_element_type=jnp.float32)
    lift_mixed = causal_conv(lift_sum.astype(jnp.bfloat16), filter_up, length)
    switch_mixed = causal_conv(switch_sum.astype(jnp.bfloat16), filter_switch, length)
    hidden = (lift_mixed * jax.nn.silu(switch_mixed)).astype(jnp.bfloat16)
    channel_partial = jnp.dot(
        hidden,
        lax.all_gather(down_weight, "fs", axis=1, tiled=True),
        preferred_element_type=jnp.float32,
    )
    channel_sum = lax.psum_scatter(
        channel_partial.astype(jnp.bfloat16), "tp", scatter_dimension=1, tiled=True
    ).astype(jnp.float32)
    return (mixed_rows.astype(jnp.float32) + channel_sum).astype(jnp.bfloat16)


def solution(mesh):
    return jax.shard_map(
        on_device,
        mesh=mesh,
        in_specs=(
            P(("grp", "fs"), "tp"),
            P(),
            P("fs", "tp"),
            P("fs", "tp"),
            P("fs", "tp"),
            P("fs", "tp"),
            P("tp"),
            P("tp", "fs"),
            P(),
            P("fs", "tp"),
            P("fs", "tp"),
            P(None, "tp"),
            P(None, "tp"),
            P("tp", "fs"),
        ),
        out_specs=P(("grp", "fs"), "tp"),
        check_vma=False,
    )
```

profile of v0, /device:TPU:3, one launch (start us, length us, event | category | flops | bytes accessed | tf_op | source)
XLA Modules:
  0.0 640.7 jit_solution(9594428033085548572)
XLA Ops:
  6.5 0.7 all-gather.11.cloned.1.call-update
  7.3 0.0 all-gather.15.cloned.1.call-start
  7.3 0.7 all-gather.15.cloned.1.call-update
  8.0 0.0 all-gather.17.cloned.1.call-start
  8.1 0.7 all-gather.17.cloned.1.call-update
  8.7 0.0 all-gather.13.cloned.1.call-start
  8.8 0.5 all-gather.13.cloned.1.call-update
  9.3 0.0 all-gather.19.cloned.1.call-start
  9.4 0.5 all-gather.19.cloned.1.call-update
  9.9 0.0 all-gather.21.cloned.1.call-start
  10.0 0.5 all-gather.21.cloned.1.call-update
  10.5 0.0 reduce-scatter.3.cloned.1.call-start
  10.6 1.6 select_convert_fusion
  12.2 1.0 iota_compare_fusion
  13.2 0.8 multiply_cosine_fusion
  14.0 24.0 %all-gather.11.cloned.1.call-done = bf16[768,2048]{1,0:T(8,128)(2,1)} async-done(((bf16[768,512]{1,0:T(8,128)(2,1)}), bf16[768,2048]{1,0:T(8,128)(2,1)}) %all-gather.11.cloned.1.call-update) | async-done | bytes 3145744 | tf_op jit(solution)/shard_map/all_gather | solution.py:100
  37.9 2.7 fusion
  40.7 0.1 copy-done
  40.8 0.8 fusion.2
  41.6 26.2 %all-gather.15.cloned.1.call-done = bf16[2048,256]{1,0:T(8,128)(2,1)} async-done(((bf16[512,256]{1,0:T(8,128)(2,1)}), bf16[2048,256]{1,0:T(8,128)(2,1)}) %all-gather.15.cloned.1.call-update) | async-done | bytes 1048592 | tf_op jit(solution)/shard_map/all_gather | solution.py:103
  67.8 2.2 convolution_convert_fusion.6
  70.0 0.1 convert.18
  70.1 26.6 %all-gather.17.cloned.1.call-done = bf16[2048,256]{1,0:T(8,128)(2,1)} async-done(((bf16[512,256]{1,0:T(8,128)(2,1)}), bf16[2048,256]{1,0:T(8,128)(2,1)}) %all-gather.17.cloned.1.call-update) | async-done | bytes 1048592 | tf_op jit(solution)/shard_map/all_gather | solution.py:104
  96.7 3.2 convolution_convert_fusion.5
  99.9 0.1 convert.19
  100.0 1.0 subtract_convert_fusion
  101.1 24.5 %all-gather.13.cloned.1.call-done = bf16[2048,256]{1,0:T(8,128)(2,1)} async-done(((bf16[512,256]{1,0:T(8,128)(2,1)}), bf16[2048,256]{1,0:T(8,128)(2,1)}) %all-gather.13.cloned.1.call-update) | async-done | bytes 1048592 | tf_op jit(solution)/shard_map/all_gather | solution.py:105
  125.5 3.2 convolution_convert_fusion.7
  128.8 0.0 copy-start.17
  128.8 4.1 multiply_reduce_fusion
  133.0 1.2 broadcast_multiply_fusion
  134.2 0.3 copy.15
  134.5 0.0 copy-start.3
  134.5 19.9 %all-gather.19.cloned.1.call-done = bf16[2048,256]{1,0:T(8,128)(2,1)} async-done(((bf16[512,256]{1,0:T(8,128)(2,1)}), bf16[2048,256]{1,0:T(8,128)(2,1)}) %all-gather.19.cloned.1.call-update) | async-done | bytes 1048592 | tf_op jit(solution)/shard_map/all_gather | solution.py:106
  154.4 28.8 %all-gather.21.cloned.1.call-done = bf16[256,2048]{1,0:T(8,128)(2,1)} async-done(((bf16[256,512]{1,0:T(8,128)(2,1)}), bf16[256,2048]{1,0:T(8,128)(2,1)}) %all-gather.21.cloned.1.call-update) | async-done | bytes 1048592 | tf_op jit(solution)/shard_map/all_gather | solution.py:119
  183.2 7.5 %convolution_convert_fusion = bf16[768,2048]{1,0:T(8,128)(2,1)} fusion(bf16[256,2048]{1,0:T(8,128)(2,1)} %all-gather.21.cloned.1.call-done, bf16[768,2048]{1,0:T(8,128)(2,1)} %copy-done.4, bf16[2048,256]{1,0:T(8,128)(2,1)} %all-gather.19.cloned.1.call-done, f32[768,256]{1,0:T(8,128)S(1)} %copy.15, f32[256]{0:T(256)S(1)} %copy-done.17), kind=kOutput, calls=%fused_computation.23 | convolution fusion | flops 1613955072 | bytes 9176064 | tf_op jit(solution)/shard_map/dot_general | solution.py:117
  190.7 0.0 reduce-scatter.3.cloned.1.call-update
  190.7 0.2 all-gather.23.cloned.1.call-start
  191.0 36.4 %reduce-scatter.3.cloned.1.call-done = bf16[768,512]{1,0:T(8,128)(2,1)} async-done(((bf16[768,2048]{1,0:T(8,128)(2,1)}), bf16[768,512]{1,0:T(8,128)(2,1)}) %reduce-scatter.3.cloned.1.call-update) | async-done | bytes 786448 | tf_op jit(solution)/shard_map/reduce_scatter | solution.py:122
  227.3 2.2 add_convert_fusion.1
  229.6 0.0 all-gather.23.cloned.1.call-update
  229.6 0.0 all-gather.27.cloned.1.call-start
  229.6 0.7 all-gather.27.cloned.1.call-update
  230.3 0.0 all-gather.25.cloned.1.call-start
  230.4 0.5 all-gather.25.cloned.1.call-update
  230.9 0.0 all-gather.29.cloned.1.call-start
  231.0 0.7 all-gather.29.cloned.1.call-update
  231.7 0.0 reduce-scatter.5.cloned.1.call-start
  231.7 0.1 slice_reduce_fusion.2
  231.8 26.8 %all-gather.23.cloned.1.call-done = bf16[768,2048]{1,0:T(8,128)(2,1)} async-done(((bf16[768,512]{1,0:T(8,128)(2,1)}), bf16[768,2048]{1,0:T(8,128)(2,1)}) %all-gather.23.cloned.1.call-update) | async-done | bytes 3145744 | tf_op jit(solution)/shard_map/all_gather | solution.py:126
  258.6 2.6 fusion.3
  261.2 106.5 %all-gather.27.cloned.1.call-done = bf16[2048,1408]{1,0:T(8,128)(2,1)} async-done(((bf16[512,1408]{1,0:T(8,128)(2,1)}), bf16[2048,1408]{1,0:T(8,128)(2,1)}) %all-gather.27.cloned.1.call-update) | async-done | bytes 5767184 | tf_op jit(solution)/shard_map/all_gather | solution.py:130
  367.7 8.6 %convolution_convert_fusion.2 = bf16[768,1408]{1,0:T(8,128)(2,1)S(1)} fusion(bf16[2048,1408]{1,0:T(8,128)(2,1)} %all-gather.27.cloned.1.call-done, bf16[768,2048]{1,0:T(8,128)(2,1)} %all-gather.23.cloned.1.call-done, f32[2048]{0:T(1024)S(1)} %copy-done.16, f32[768]{0:T(1024)S(1)} %add_rsqrt_fusion.1), kind=kOutput, calls=%fused_computation.25 | convolution fusion | flops 4436557824 | bytes 11086848 | tf_op jit(solution)/shard_map/dot_general | solution.py:134
  376.3 1.4 copy-done.6
  377.7 2.5 convert_bitcast_fusion
  380.2 93.9 %all-gather.25.cloned.1.call-done = bf16[2048,1408]{1,0:T(8,128)(2,1)} async-done(((bf16[512,1408]{1,0:T(8,128)(2,1)}), bf16[2048,1408]{1,0:T(8,128)(2,1)}) %all-gather.25.cloned.1.call-update) | async-done | bytes 5767184 | tf_op jit(solution)/shard_map/all_gather | solution.py:129
  474.1 8.0 %convolution_convert_fusion.3 = bf16[768,1408]{1,0:T(8,128)(2,1)S(1)} fusion(bf16[2048,1408]{1,0:T(8,128)(2,1)} %all-gather.25.cloned.1.call-done, bf16[768,2048]{1,0:T(8,128)(2,1)S(1)} %copy-done.2, f32[2048]{0:T(1024)S(1)} %copy-done.16, f32[768]{0:T(1024)S(1)} %add_rsqrt_fusion.1), kind=kOutput, calls=%fused_computation.26 | convolution fusion | flops 4436557824 | bytes 11086848 | tf_op jit(solution)/shard_map/dot_general | solution.py:133
  482.2 1.3 copy-done.8
  483.5 2.4 convert_bitcast_fusion.1
  485.9 94.8 %all-gather.29.cloned.1.call-done = bf16[1408,2048]{1,0:T(8,128)(2,1)} async-done(((bf16[1408,512]{1,0:T(8,128)(2,1)}), bf16[1408,2048]{1,0:T(8,128)(2,1)}) %all-gather.29.cloned.1.call-update) | async-done | bytes 5767184 | tf_op jit(solution)/shard_map/all_gather | solution.py:140
  580.7 16.0 %convolution_convert_fusion.1 = bf16[768,2048]{1,0:T(8,128)(2,1)} fusion(bf16[1408,2048]{1,0:T(8,128)(2,1)} %all-gather.29.cloned.1.call-done, bf16[768,1408]{1,0:T(8,128)(2,1)} %copy-done.8, bf16[768,1408]{1,0:T(8,128)(2,1)S(1)} %copy-done.7, f32[1,768,1408]{2,1,0:T(8,128)} %convert_bitcast_fusion, f32[1,768,1408]{2,1,0:T(8,128)} %convert_bitcast_fusion.1, ...), kind=kOutput, calls=%fused_computation.24 | convolution fusion | flops 4450222080 | bytes 21922816 | tf_op jit(solution)/shard_map/dot_general | solution.py:138
  596.7 0.0 reduce-scatter.5.cloned.1.call-update
  596.7 34.9 %reduce-scatter.5.cloned.1.call-done = bf16[768,512]{1,0:T(8,128)(2,1)} async-done(((bf16[768,2048]{1,0:T(8,128)(2,1)}), bf16[768,512]{1,0:T(8,128)(2,1)}) %reduce-scatter.5.cloned.1.call-update) | async-done | bytes 786448 | tf_op jit(solution)/shard_map/reduce_scatter | solution.py:143
  631.6 2.2 add_convert_fusion
  (38 shorter events, 0.1 us)
Async XLA Ops:
  6.5 34.1 %copy-start.15 = (f32[2048]{0:T(1024)S(1)}, f32[2048]{0:T(1024)}, u32[]{:S(2)}) copy-start(f32[2048]{0:T(1024)} %param.15) | copy-start | bytes 24580
  6.5 31.4 %all-gather.11.cloned.1.call-start = ((), (), s32[]{:S(2)}) async-start(), calls=%async_computation.2 | async-start | bytes 3932160 | tf_op jit(solution)/shard_map/all_gather | solution.py:100
  7.3 60.5 %all-gather.15.cloned.1.call-start = ((), (), s32[]{:S(2)}) async-start(), calls=%async_computation.4 | async-start | bytes 1310720 | tf_op jit(solution)/shard_map/all_gather | solution.py:103
  8.0 88.7 %all-gather.17.cloned.1.call-start = ((), (), s32[]{:S(2)}) async-start(), calls=%async_computation.5 | async-start | bytes 1310720 | tf_op jit(solution)/shard_map/all_gather | solution.py:104
  8.7 116.8 %all-gather.13.cloned.1.call-start = ((), (), s32[]{:S(2)}) async-start(), calls=%async_computation.3 | async-start | bytes 1310720 | tf_op jit(solution)/shard_map/all_gather | solution.py:105
  9.3 145.0 %all-gather.19.cloned.1.call-start = ((), (), s32[]{:S(2)}) async-start(), calls=%async_computation.6 | async-start | bytes 1310720 | tf_op jit(solution)/shard_map/all_gather | solution.py:106
  9.9 173.3 %all-gather.21.cloned.1.call-start = ((), (), s32[]{:S(2)}) async-start(), calls=%async_computation.7 | async-start | bytes 1310720 | tf_op jit(solution)/shard_map/all_gather | solution.py:119
  10.5 216.9 %reduce-scatter.3.cloned.1.call-start = ((), (), s32[]{:S(2)}) async-start(), calls=%async_computation.8 | async-start | bytes 3932160 | tf_op jit(solution)/shard_map/reduce_scatter | solution.py:122
  37.9 2.8 copy-start
  41.6 28.4 %copy-start.4 = (bf16[768,2048]{1,0:T(8,128)(2,1)}, bf16[768,2048]{1,0:T(8,128)(2,1)S(1)}, u32[]{:S(2)}) copy-start(bf16[768,2048]{1,0:T(8,128)(2,1)S(1)} %fusion.2) | copy-start | bytes 9437188
  100.0 28.8 %copy-start.5 = (f32[768,768]{1,0:T(8,128)S(1)}, f32[768,768]{1,0:T(8,128)}, u32[]{:S(2)}) copy-start(f32[768,768]{1,0:T(8,128)} %select_convert_fusion) | copy-start | bytes 7077892
  101.0 27.7 %copy-start.9 = (bf16[768,2,64]{0,2,1:T(8,128)(2,1)S(1)}, bf16[768,2,64]{0,2,1:T(8,128)(2,1)}, u32[]{:S(2)}) copy-start(bf16[768,2,64]{0,2,1:T(8,128)(2,1)} %get-tuple-element.11) | copy-start | bytes 589828
  101.0 27.7 %copy-start.10 = (bf16[768,2,64]{0,2,1:T(8,128)(2,1)S(1)}, bf16[768,2,64]{0,2,1:T(8,128)(2,1)}, u32[]{:S(2)}) copy-start(bf16[768,2,64]{0,2,1:T(8,128)(2,1)} %get-tuple-element.12) | copy-start | bytes 589828
  101.1 27.7 %copy-start.11 = (bf16[768,2,64]{0,2,1:T(8,128)(2,1)S(1)}, bf16[768,2,64]{0,2,1:T(8,128)(2,1)}, u32[]{:S(2)}) copy-start(bf16[768,2,64]{0,2,1:T(8,128)(2,1)} %get-tuple-element.15) | copy-start | bytes 589828
  101.1 27.7 %copy-start.12 = (bf16[768,2,64]{0,2,1:T(8,128)(2,1)S(1)}, bf16[768,2,64]{0,2,1:T(8,128)(2,1)}, u32[]{:S(2)}) copy-start(bf16[768,2,64]{0,2,1:T(8,128)(2,1)} %get-tuple-element.16) | copy-start | bytes 589828
  128.8 54.4 %copy-start.17 = (f32[256]{0:T(256)S(1)}, f32[256]{0:T(256)}, u32[]{:S(2)}) copy-start(f32[256]{0:T(256)} %param.20) | copy-start | bytes 3076
  134.5 92.9 %copy-start.3 = (bf16[768,512]{1,0:T(8,128)(2,1)S(1)}, bf16[768,512]{1,0:T(8,128)(2,1)}, u32[]{:S(2)}) copy-start(bf16[768,512]{1,0:T(8,128)(2,1)} %param.14) | copy-start | bytes 2359300
  190.7 41.0 %copy-start.13 = (f32[3,1408]{1,0:T(4,128)S(1)}, f32[3,1408]{1,0:T(4,128)}, u32[]{:S(2)}) copy-start(f32[3,1408]{1,0:T(4,128)} %param.26) | copy-start | bytes 50692
  190.7 41.0 %copy-start.14 = (f32[3,1408]{1,0:T(4,128)S(1)}, f32[3,1408]{1,0:T(4,128)}, u32[]{:S(2)}) copy-start(f32[3,1408]{1,0:T(4,128)} %param.25) | copy-start | bytes 50692
  190.7 67.9 %all-gather.23.cloned.1.call-start = ((), (), s32[]{:S(2)}) async-start(), calls=%async_computation.9 | async-start | bytes 3932160 | tf_op jit(solution)/shard_map/all_gather | solution.py:126
  229.6 138.2 %copy-start.16 = (f32[2048]{0:T(1024)S(1)}, f32[2048]{0:T(1024)}, u32[]{:S(2)}) copy-start(f32[2048]{0:T(1024)} %param.22) | copy-start | bytes 24580
  229.6 138.1 %all-gather.27.cloned.1.call-start = ((), (), s32[]{:S(2)}) async-start(), calls=%async_computation.11 | async-start | bytes 7208960 | tf_op jit(solution)/shard_map/all_gather | solution.py:130
  230.3 243.8 %all-gather.25.cloned.1.call-start = ((), (), s32[]{:S(2)}) async-start(), calls=%async_computation.10 | async-start | bytes 7208960 | tf_op jit(solution)/shard_map/all_gather | solution.py:129
  230.9 349.8 %all-gather.29.cloned.1.call-start = ((), (), s32[]{:S(2)}) async-start(), calls=%async_computation.12 | async-start | bytes 7208960 | tf_op jit(solution)/shard_map/all_gather | solution.py:140
  231.7 400.0 %reduce-scatter.5.cloned.1.call-start = ((), (), s32[]{:S(2)}) async-start(), calls=%async_computation.13 | async-start | bytes 3932160 | tf_op jit(solution)/shard_map/reduce_scatter | solution.py:143
  376.3 1.4 copy-start.6
  377.7 96.4 %copy-start.2 = (bf16[768,2048]{1,0:T(8,128)(2,1)S(1)}, bf16[768,2048]{1,0:T(8,128)(2,1)}, u32[]{:S(2)}) copy-start(bf16[768,2048]{1,0:T(8,128)(2,1)} %all-gather.23.cloned.1.call-done) | copy-start | bytes 9437188
  482.2 1.4 copy-start.8
  483.5 97.1 %copy-start.7 = (bf16[768,1408]{1,0:T(8,128)(2,1)S(1)}, bf16[768,1408]{1,0:T(8,128)(2,1)}, u32[]{:S(2)}) copy-start(bf16[768,1408]{1,0:T(8,128)(2,1)} %copy-done.6) | copy-start | bytes 6488068
  580.7 50.9 %copy-start.1 = (bf16[768,512]{1,0:T(8,128)(2,1)S(1)}, bf16[768,512]{1,0:T(8,128)(2,1)}, u32[]{:S(2)}) copy-start(bf16[768,512]{1,0:T(8,128)(2,1)} %add_convert_fusion.1) | copy-start | bytes 2359300
Sparse Core Ops, SparseCore 0:
  8.9 28.9 all-gather.10
  39.5 28.2 all-gather.14
  69.3 27.3 all-gather.16
  98.2 27.3 all-gather.12
  127.0 27.3 all-gather.18
  155.8 27.3 all-gather.20
  190.8 36.4 reduce-scatter.2
  229.7 28.8 all-gather.22
  260.2 107.4 all-gather.26
  369.1 104.9 all-gather.24
  475.7 104.9 all-gather.28
  596.8 34.7 reduce-scatter.4
where the time goes:
time: 644 us; the launch traced here: 641 us
  waiting for transfers between devices  549 us (85%)
  matrix products  52.9 us (8%)
  other arithmetic  21.2 us (3%)
  between operations  13.8 us (2%)
    all_gather x1, waiting for transfers between devices, on_device(): lax.all_gather(switch_weight, 'fs', axis=0, tiled=True)  107 us
    all_gather x1, waiting for transfers between devices, on_device(): lax.all_gather(down_weight, 'fs', axis=1, tiled=True)  94.8 us
    all_gather x1, waiting for transfers between devices, on_device(): lax.all_gather(up_weight, 'fs', axis=0, tiled=True)  93.9 us
    reduce_scatter x1, waiting for transfers between devices, on_device(): lax.psum_scatter(partial_value.astype(jnp.bfloat16), 'tp', scatter_dimens...  36.4 us
    reduce_scatter x1, waiting for transfers between devices, on_device(): lax.psum_scatter(channel_partial.astype(jnp.bfloat16), 'tp', scatter_dime...  34.9 us
    all_gather x1, waiting for transfers between devices, on_device(): lax.all_gather(out_weight, 'fs', axis=1, tiled=True)  28.8 us
    all_gather x1, waiting for transfers between devices, on_device(): mixed_whole = lax.all_gather(mixed_rows, 'tp', axis=1, tiled=True)  26.8 us
    all_gather x1, waiting for transfers between devices, on_device(): lax.all_gather(key_weight, 'fs', axis=0, tiled=True)  26.6 us
  transfers between devices with their start and end apart: 12, of which 12 were waited for; matrix products, arithmetic and copies ran while one was open for 7% of the time, Pallas kernels for 0%

commit v1 on v0

v1 whole, which is shorter than its diff:
```python
import functools

import jax
import jax.numpy as jnp
from jax import lax
from jax.experimental import pallas as pl
from jax.experimental.pallas import tpu as pltpu
from jax.sharding import PartitionSpec as P

HEAD = 128
EPS = 1e-06
MESH = pl.DeviceIdType.MESH
BF = jnp.bfloat16
F32 = jnp.float32


def chunks_of(rows):
    return 2 if rows % 32 == 0 else 1


def kernel(cfg, x_hbm, mg, q_hbm, k_hbm, v_hbm, g_hbm, hg, ow_hbm, cg, up_hbm, sw_hbm, fu, fsw, dn_hbm,
           cos_ref, sin_ref, ld_ref, o_ref,
           wq, ob, ub, sb, db, xw, xn, qr, kr, vr, gr, ho, part, ra, st, rb, mw, lift, swit, hid,
           part2, ra2, st2, rb2,
           loc, zs, zr, ys, yr, a1s, a1r, a2s, a2r, b1s, b1r, b2s, b2r, c1s, c1r, c2s, c2r, d1s, d1r, d2s, d2r):
    n_g, n_f, n_t = cfg
    n_x = n_t // 2
    grp, z, t = lax.axis_index("grp"), lax.axis_index("fs"), lax.axis_index("tp")
    x, c = t // 2, t % 2
    partner = x * 2 + (1 - c)
    T, bw = x_hbm.shape
    D = bw * n_t
    RC = 256
    R = T // RC
    width = q_hbm.shape[1]
    heads = width // HEAD
    F = up_hbm.shape[1]
    fr = q_hbm.shape[0]
    slotw = ow_hbm.shape[1]
    per_block = bw // slotw

    def rows_of(r, size=RC):
        return pl.ds(r * size if isinstance(r, int) else pl.multiple_of(r * size, size), size)

    barrier = pltpu.get_barrier_semaphore()
    friends = [(grp, lax.rem(z + 1, n_f), t), (grp, lax.rem(z + n_f - 1, n_f), t), (grp, z, partner)]
    friends += [(lax.rem(grp + d, n_g), z, t) for d in range(1, n_g)]
    friends += [(grp, z, lax.rem(x + d, n_x) * 2 + c) for d in range(1, n_x)]
    for f in friends:
        pl.semaphore_signal(barrier, inc=1, device_id=f, device_id_type=MESH)

    zrow = pl.multiple_of(z * fr, fr)
    local = [pltpu.make_async_copy(x_hbm, xw.at[t], loc.at[0])]
    for i, w in enumerate((q_hbm, k_hbm, v_hbm, g_hbm)):
        local.append(pltpu.make_async_copy(
            w, wq.at[pl.ds(zrow, fr), pl.ds(i * width, width)], loc.at[1 + i]))
    local.append(pltpu.make_async_copy(ow_hbm, ob.at[z], loc.at[5]))
    local.append(pltpu.make_async_copy(up_hbm, ub.at[pl.ds(zrow, fr), :], loc.at[6]))
    local.append(pltpu.make_async_copy(sw_hbm, sb.at[pl.ds(zrow, fr), :], loc.at[7]))
    local.append(pltpu.make_async_copy(dn_hbm, db.at[z], loc.at[8]))
    for cp in local:
        cp.start()

    pending = []

    pieces = []

    def add_pieces(buf, slotted, shard, name):
        half = shard // n_g
        count = 1 if name == "out" else chunks_of(half)
        size = half // count
        for j in range(count):
            def ref(src, owner, j=j):
                if slotted:
                    lo = owner * half + j * size
                    return buf.at[src, pl.ds(pl.multiple_of(lo, size), size), :]
                lo = src * shard + owner * half + j * size
                return buf.at[pl.ds(pl.multiple_of(lo, size), size), :]
            pieces.append((name, ref))

    add_pieces(wq, False, fr, "qkvg")
    add_pieces(ob, True, ow_hbm.shape[0], "out")
    add_pieces(ub, False, fr, "up")
    add_pieces(sb, False, fr, "switch")
    add_pieces(db, True, dn_hbm.shape[0], "down")
    n_p = len(pieces)

    def z_copy(p, src, step, way):
        ref = pieces[p][1](src, grp)
        return pltpu.make_async_remote_copy(
            src_ref=ref, dst_ref=ref, send_sem=zs.at[p, 2 * step + way], recv_sem=zr.at[p, src],
            device_id=(grp, z + (1 if way == 0 else -1), t), device_id_type=MESH)

    def y_copy(p, src, d):
        ref = pieces[p][1](src, grp)
        return pltpu.make_async_remote_copy(
            src_ref=ref, dst_ref=ref, send_sem=ys.at[p, src * n_g + d], recv_sem=yr.at[p, src * n_g + grp],
            device_id=(lax.rem(grp + d, n_g), z, t), device_id_type=MESH)

    def z_send(p, src, step, way, cond):
        cp = z_copy(p, src, step, way)

        @pl.when(cond)
        def _():
            cp.start()

        pending.append((cond, cp))

    def own(p):
        z_send(p, z, 0, 0, z < n_f - 1)
        z_send(p, z, 0, 1, z > 0)

    def event(p, s):
        for way in (0, 1):
            src = z - s if way == 0 else z + s
            here = (src >= 0) if way == 0 else (src < n_f)
            safe = jnp.clip(src, 0, n_f - 1)

            @pl.when(here)
            def _():
                z_copy(p, safe, s, way).wait_recv()

            onward = jnp.logical_and(here, z < n_f - 1 if way == 0 else z > 0)
            z_send(p, safe, s, way, onward)
            for d in range(1, n_g):
                cp = y_copy(p, safe, d)

                @pl.when(here)
                def _():
                    cp.start()

                pending.append((here, cp))

    def arrive(p):
        for s in range(1, n_f):
            src = lax.rem(z + s, n_f)
            for d in range(1, n_g):
                owner = lax.rem(grp + d, n_g)
                ref = pieces[p][1](src, owner)
                pltpu.make_async_remote_copy(
                    src_ref=ref, dst_ref=ref, send_sem=ys.at[p, src * n_g],
                    recv_sem=yr.at[p, src * n_g + owner],
                    device_id=(owner, z, t), device_id_type=MESH).wait_recv()

    state = {"own": 0, "ev": 0}
    order = [(p, s) for p in range(n_p) for s in range(1, n_f)]

    def send_own(upto):
        while state["own"] < min(upto, n_p):
            own(state["own"])
            state["own"] += 1

    def pump(count=1):
        for _ in range(count):
            if state["ev"] < len(order):
                p, s = order[state["ev"]]
                send_own(p + 2)
                event(p, s)
                state["ev"] += 1

    def pump_through(name):
        last = max(i for i, pc in enumerate(pieces) if pc[0] == name)
        while state["ev"] < len(order) and order[state["ev"]][0] <= last:
            pump()

    def arrive_all(name):
        pump_through(name)
        for i, pc in enumerate(pieces):
            if pc[0] == name:
                arrive(i)

    def ag_copy(buf, src_x, r, dest, ssem, rsem):
        ref = buf.at[src_x * 2 + c, rows_of(r), :]
        return pltpu.make_async_remote_copy(
            src_ref=ref, dst_ref=ref, send_sem=ssem, recv_sem=rsem,
            device_id=(grp, z, dest), device_id_type=MESH)

    def go(cp):
        cp.start()
        pending.append((None, cp))

    def ag_start(buf, r, sems):
        s1, r1, s2, r2 = sems
        for d in range(1, n_x):
            go(ag_copy(buf, x, r, lax.rem(x + d, n_x) * 2 + c, s1.at[d, r], r1.at[x, r]))
        go(ag_copy(buf, x, r, partner, s2.at[x, r], r2.at[x, r]))

    def ag_forward(buf, r, sems):
        s1, r1, s2, r2 = sems
        for d in range(1, n_x):
            sx = lax.rem(x + d, n_x)
            ag_copy(buf, sx, r, partner, s1.at[d, r], r1.at[sx, r]).wait_recv()
            go(ag_copy(buf, sx, r, partner, s2.at[sx, r], r2.at[sx, r]))

    def ag_finish(buf, r, sems):
        s1, r1, s2, r2 = sems
        for sx in range(n_x):
            ref = buf.at[sx * 2 + (1 - c), rows_of(r), :]
            pltpu.make_async_remote_copy(
                src_ref=ref, dst_ref=ref, send_sem=s2.at[sx, r], recv_sem=r2.at[sx, r],
                device_id=(grp, z, partner), device_id_type=MESH).wait_recv()

    def norm_rows(src, gain, r):
        def body(i, _):
            rows = rows_of(r * (RC // 64) + i, 64)
            total = jnp.zeros((64, 1), F32)
            for b in range(n_t):
                val = src[b, rows, :].astype(F32)
                total = total + jnp.sum(val * val, axis=-1, keepdims=True)
            inv = lax.rsqrt(total / D + EPS)
            for b in range(n_t):
                val = src[b, rows, :].astype(F32)
                xn[rows, b * bw:(b + 1) * bw] = (val * inv * gain[:, b * bw:(b + 1) * bw]).astype(BF)
            return 0
        lax.fori_loop(0, RC // 64, body, 0)

    def product(lhs, rhs, dst, block, r):
        for j in range(per_block):
            dst[block, rows_of(r), j * slotw:(j + 1) * slotw] = jnp.dot(
                lhs[rows_of(r), :], rhs[block * per_block + j], preferred_element_type=F32).astype(BF)

    def rs_copy(src_ref, dst_ref, dest, ssem, rsem):
        return pltpu.make_async_remote_copy(
            src_ref=src_ref, dst_ref=dst_ref, send_sem=ssem, recv_sem=rsem,
            device_id=(grp, z, dest), device_id_type=MESH)

    def reduce(lhs, rhs, prt, r_a, stage, r_b, sems, base, emit, between):
        s1, r1, s2, r2 = sems

        def to_partner(d, r):
            bx = lax.rem(x + d, n_x)
            return rs_copy(prt.at[bx * 2 + 1 - c, rows_of(r), :], r_a.at[d, rows_of(r), :],
                           partner, s1.at[d, r], r1.at[d, r])

        def across(d, r):
            return rs_copy(stage.at[d, rows_of(r), :], r_b.at[d, rows_of(r), :],
                           lax.rem(x + d, n_x) * 2 + c, s2.at[d, r], r2.at[d, r])

        def combine(d, r):
            bx = lax.rem(x + d, n_x)
            to_partner(d, r).wait_recv()
            stage[d, rows_of(r), :] = (prt[bx * 2 + c, rows_of(r), :].astype(F32)
                                       + r_a[d, rows_of(r), :].astype(F32)).astype(BF)
            go(across(d, r))

        work = [(d, r) for d in range(1, n_x) for r in range(R)]
        prev = None
        for d, r in work + [(0, r) for r in range(R)]:
            bx = lax.rem(x + d, n_x)
            product(lhs, rhs, prt, bx * 2 + 1 - c, r)
            go(to_partner(d, r))
            product(lhs, rhs, prt, bx * 2 + c, r)
            if prev is not None and prev[0] > 0:
                combine(*prev)
            prev = (d, r)
            between()
        for r in range(R):
            to_partner(0, r).wait_recv()
            total = prt[t, rows_of(r), :].astype(F32) + r_a[0, rows_of(r), :].astype(F32)
            for d in range(1, n_x):
                across(d, r).wait_recv()
                total = total + r_b[d, rows_of(r), :].astype(F32)
            emit(r, (base[t, rows_of(r), :].astype(F32) + total).astype(BF))

    pl.semaphore_wait(barrier, len(friends))
    local[0].wait()
    agx = (a1s, a1r, a2s, a2r)
    for r in range(R):
        ag_start(xw, r, agx)
    for cp in local[1:]:
        cp.wait()
    send_own(2)
    pump(1)
    for r in range(R):
        ag_forward(xw, r, agx)
    pump(1)
    for r in range(R):
        ag_finish(xw, r, agx)
        norm_rows(xw, mg, r)
        pump(1)
    arrive_all("qkvg")
    send_own(5)

    def project(r, _):
        rows = rows_of(r)
        lhs = xn[rows, :]
        for i, dst in enumerate((qr, kr, vr, gr)):
            val = jnp.dot(lhs, wq[:, i * width:(i + 1) * width], preferred_element_type=F32).astype(BF)
            if i >= 2:
                dst[rows, :] = val
                continue
            for h in range(heads):
                part_h = val[:, h * HEAD:(h + 1) * HEAD].astype(F32)
                dst[rows, h * HEAD:(h + 1) * HEAD] = (
                    part_h * cos_ref[rows, :] + pltpu.roll(part_h, HEAD // 2, 1) * sin_ref[rows, :]).astype(BF)
        return 0

    lax.fori_loop(0, R, project, 0)
    pump(2)
    for h in range(heads):
        cols = slice(h * HEAD, (h + 1) * HEAD)
        for r in range(R):
            span = (r + 1) * RC
            qh = qr[r * RC:(r + 1) * RC, cols]
            scores = lax.dot_general(qh, kr[0:span, cols], (((1,), (1,)), ((), ())),
                                     preferred_element_type=F32)
            gap = (r * RC + lax.broadcasted_iota(jnp.int32, (RC, span), 0)
                   - lax.broadcasted_iota(jnp.int32, (RC, span), 1))
            causal = gap >= 0
            rate = ld_ref[h:h + 1, 0:1]
            fade = jnp.where(causal, jnp.exp(rate * jnp.where(causal, gap, 0).astype(F32)), 0.0)
            weights = (scores * HEAD ** (-0.5) * fade).astype(BF)
            kept = jnp.dot(weights, vr[0:span, cols], preferred_element_type=F32)
            kept = kept * lax.rsqrt(jnp.mean(kept * kept, axis=-1, keepdims=True) + EPS)
            gate = gr[r * RC:(r + 1) * RC, cols].astype(F32)
            ho[r * RC:(r + 1) * RC, cols] = (kept * hg[:, cols] * (gate / (1.0 + jnp.exp(-gate)))).astype(BF)
    arrive_all("out")
    send_own(6)
    agm = (c1s, c1r, c2s, c2r)

    def emit_mixed(r, val):
        mw[t, rows_of(r), :] = val
        ag_start(mw, r, agm)

    reduce(ho, ob, part, ra, st, rb, (b1s, b1r, b2s, b2r), xw, emit_mixed, lambda: None)
    pump(1)
    for r in range(R):
        ag_forward(mw, r, agm)
    pump(1)
    for r in range(R):
        ag_finish(mw, r, agm)
        norm_rows(mw, cg, r)
    arrive_all("up")

    lift[0:16, :] = jnp.zeros((16, F), BF)
    swit[0:16, :] = jnp.zeros((16, F), BF)

    def widen(weights, dst, r):
        dst[pl.ds(16 + r * RC, RC), :] = jnp.dot(
            xn[rows_of(r), :], weights[...], preferred_element_type=F32).astype(BF)

    for r in range(R):
        widen(ub, lift, r)
        pump(1)
    arrive_all("switch")
    edges = list(range(0, F, 256)) + [F]

    def conv_rows(i, _):
        for lo, hi in zip(edges[:-1], edges[1:]):
            mixed = []
            for src, taps in ((lift, fu), (swit, fsw)):
                val = src[pl.ds(pl.multiple_of(i * 64, 64), 80), lo:hi].astype(F32)
                acc = pltpu.roll(val, 2, 0)[16:] * taps[0:1, lo:hi]
                acc = acc + pltpu.roll(val, 1, 0)[16:] * taps[1:2, lo:hi]
                mixed.append(acc + val[16:] * taps[2:3, lo:hi])
            a, b = mixed
            hid[rows_of(i, 64), lo:hi] = (a * (b / (1.0 + jnp.exp(-b)))).astype(BF)
        return 0

    for r in range(R):
        widen(sb, swit, r)
        lax.fori_loop(r * (RC // 64), (r + 1) * (RC // 64), conv_rows, 0)
        pump(1)
    arrive_all("down")

    def emit_out(r, val):
        o_ref[rows_of(r), :] = val

    reduce(hid, db, part2, ra2, st2, rb2, (d1s, d1r, d2s, d2r), mw, emit_out, lambda: None)

    for cond, cp in pending:
        if cond is None:
            cp.wait_send()
        else:
            @pl.when(cond)
            def _(cp=cp):
                cp.wait_send()


def on_device(cfg, inputs, mixer_gain, query_weight, key_weight, value_weight, gate_weight, head_gain,
              out_weight, channel_gain, up_weight, switch_weight, filter_up, filter_switch, down_weight):
    n_g, n_f, n_t = cfg
    n_x = n_t // 2
    T, bw = inputs.shape
    D = bw * n_t
    fr, width = query_weight.shape
    heads = width // HEAD
    F = up_weight.shape[1]
    slotw = out_weight.shape[1]
    half = HEAD // 2
    frequency = 10000.0 ** (-jnp.arange(half, dtype=F32) * 2.0 / HEAD)
    angles = jnp.arange(T, dtype=jnp.int32).astype(F32)[:, None] * frequency[None, :]
    cosine, sine = jnp.cos(angles), jnp.sin(angles)
    cos2 = jnp.concatenate([cosine, cosine], axis=1)
    sin2 = jnp.concatenate([-sine, sine], axis=1)
    ids = (lax.axis_index("tp") * heads + jnp.arange(heads, dtype=jnp.int32)).astype(F32)
    rate = jnp.broadcast_to(jnp.log1p(-jnp.exp2(-5.0 - ids))[:, None], (heads, 128))

    n_p = (chunks_of(fr // n_g) * 3 + 1 + chunks_of(down_weight.shape[0] // n_g))
    R = T // 256
    dma = pltpu.SemaphoreType.DMA
    anyspec = pl.BlockSpec(memory_space=pl.ANY)
    vspec = pl.BlockSpec(memory_space=pltpu.VMEM)
    tp_sems = [dma((n_x, R))] * 16
    act = pltpu.VMEM((n_t, T, bw), BF)
    xblk = pltpu.VMEM((n_x, T, bw), BF)
    scratch = [
        pltpu.VMEM((D, 4 * width), BF),
        pltpu.VMEM((n_f,) + out_weight.shape, BF),
        pltpu.VMEM((D, F), BF),
        pltpu.VMEM((D, F), BF),
        pltpu.VMEM((n_f,) + down_weight.shape, BF),
        act,
        pltpu.VMEM((T, D), BF),
        pltpu.VMEM((T, width), BF), pltpu.VMEM((T, width), BF),
        pltpu.VMEM((T, width), BF), pltpu.VMEM((T, width), BF),
        pltpu.VMEM((T, width), BF),
        act, xblk, xblk, xblk,
        act,
        pltpu.VMEM((T + 16, F), BF), pltpu.VMEM((T + 16, F), BF), pltpu.VMEM((T, F), BF),
        act, xblk, xblk, xblk,
        dma((9,)),
        dma((n_p, 2 * n_f)), dma((n_p, n_f)), dma((n_p, n_f * n_g)), dma((n_p, n_f * n_g)),
    ] + tp_sems
    flops = 2 * T * (D * 4 * width + width * D + 3 * D * F)
    call = pl.pallas_call(
        functools.partial(kernel, cfg),
        out_shape=jax.ShapeDtypeStruct((T, bw), BF),
        in_specs=[anyspec, vspec, anyspec, anyspec, anyspec, anyspec, vspec, anyspec, vspec, anyspec, anyspec,
                  vspec, vspec, anyspec, vspec, vspec, vspec],
        out_specs=vspec,
        scratch_shapes=scratch,
        compiler_params=pltpu.CompilerParams(
            collective_id=0, has_side_effects=True, vmem_limit_bytes=67043328),
        cost_estimate=pl.CostEstimate(flops=flops, bytes_accessed=2 * (D * F * 3), transcendentals=0),
    )
    return call(inputs, mixer_gain[None, :], query_weight, key_weight, value_weight, gate_weight,
                head_gain[None, :], out_weight, channel_gain[None, :], up_weight, switch_weight,
                filter_up, filter_switch, down_weight, cos2, sin2, rate)


def solution(mesh):
    cfg = (mesh.shape["grp"], mesh.shape["fs"], mesh.shape["tp"])
    return jax.shard_map(
        functools.partial(on_device, cfg),
        mesh=mesh,
        in_specs=(
            P(("grp", "fs"), "tp"),
            P(),
            P("fs", "tp"),
            P("fs", "tp"),
            P("fs", "tp"),
            P("fs", "tp"),
            P("tp"),
            P("tp", "fs"),
            P(),
            P("fs", "tp"),
            P("fs", "tp"),
            P(None, "tp"),
            P(None, "tp"),
            P("tp", "fs"),
        ),
        out_specs=P(("grp", "fs"), "tp"),
        check_vma=False,
    )
```

time: 644 us -> 286 us (0.44)
  waiting for transfers between devices: 549 us -> 0 us
  Pallas kernels: 0 us -> 278 us
  matrix products: 52.9 us -> 0 us
  other arithmetic: 21.2 us -> 2.62 us
  between operations: 13.8 us -> 0.02 us
    all_gather x10 -> x0, waiting for transfers between devices: 472 us -> none  [the longest x1 107 us: on_device(): lax.all_gather(switch_weight, 'fs', axis=0, tiled=True)]
    pallas_call x0 -> x1, Pallas kernels: none -> 278 us  [on_device(): call(inputs, mixer_gain[None, :], query_weight, key_weight, value_weight,...]
    reduce_scatter x2 -> x0, waiting for transfers between devices: 71.3 us -> none  [the longest x1 36.4 us: on_device(): lax.psum_scatter(partial_value.astype(jnp.bfloat16), 'tp', scatter_dimens...]
    dot_general x8 -> x0, matrix products: 52.9 us -> none  [the longest x1 16 us: on_device(): jnp.dot(hidden, lax.all_gather(down_weight, 'fs', axis=1, tiled=True), pr...]
    convert_element_type x5 -> x1, other arithmetic: 6.87 us -> 0.01 us  [on_device(): jnp.arange(T, dtype=jnp.int32).astype(F32)[:, None] * frequency[None, :]]
  transfers between devices with their start and end apart: 12 -> 0, of which waited for: 12 -> 0; matrix products, arithmetic and copies ran while one was open for 7% -> 0% of each run, Pallas kernels for 0% -> 0%
where the time goes in v1:
time: 286 us; the launch traced here: 284 us
  Pallas kernels  278 us (97%)
    pallas_call x1, Pallas kernels, on_device(): call(inputs, mixer_gain[None, :], query_weight, key_weight, value_weight,...  278 us

profile of v1, /device:TPU:3, one launch (start us, length us, event | category | flops | bytes accessed | tf_op | source)
XLA Modules:
  0.0 283.7 jit_solution(14535842616660798907)
XLA Ops:
  0.0 1.5 fusion
  1.5 1.1 pad_maximum_fusion
  2.6 0.6 broadcast_in_dim.20.ld_ref
  3.2 278.4 %shard_map.136 = bf16[768,512]{1,0:T(8,128)(2,1)} custom-call(bf16[768,512]{1,0:T(8,128)(2,1)} %x_hbm.1, f32[1,2048]{1,0:T(1,128)} %bitcast.3, bf16[512,256]{1,0:T(8,128)(2,1)} %q_hbm.1, bf16[512,256]{1,0:T(8,128)(2,1)} %k_hbm.1, bf16[512,256]{1,0:T(8,128)(2,1)} %v_hbm.1, bf16[512,256]{1,0:T(8,128)(2,1)} %g_hbm.1, f32[1,256]{1,0:T(1,128)} %bitcast.5, ...), custom_call_target="tpu_custom_call" | custom-call | flops 17314086912 | bytes 17301504 | tf_op jit(solution)/shard_map/pallas_call | solution.py:437
  281.7 2.1 copy.16
  (3 shorter events, 0.0 us)

commit v2 on v1

--- a/solution.py
+++ b/solution.py
@@ -14,8 +14,10 @@
 F32 = jnp.float32
 
 
-def chunks_of(rows):
-    return 2 if rows % 32 == 0 else 1
+def chunks_of(rows, most=2):
+    while rows % (16 * most):
+        most //= 2
+    return most
 
 
 def kernel(cfg, x_hbm, mg, q_hbm, k_hbm, v_hbm, g_hbm, hg, ow_hbm, cg, up_hbm, sw_hbm, fu, fsw, dn_hbm,
@@ -67,7 +69,7 @@
 
     def add_pieces(buf, slotted, shard, name):
         half = shard // n_g
-        count = 1 if name == "out" else chunks_of(half)
+        count = 1 if name == "out" else chunks_of(half, 4 if name == "down" else 2)
         size = half // count
         for j in range(count):
             def ref(src, owner, j=j):
@@ -131,19 +133,25 @@
 
                 pending.append((here, cp))
 
+    def arrive_from(p, src):
+        for d in range(1, n_g):
+            owner = lax.rem(grp + d, n_g)
+            ref = pieces[p][1](src, owner)
+            pltpu.make_async_remote_copy(
+                src_ref=ref, dst_ref=ref, send_sem=ys.at[p, src * n_g],
+                recv_sem=yr.at[p, src * n_g + owner],
+                device_id=(owner, z, t), device_id_type=MESH).wait_recv()
+
     def arrive(p):
         for s in range(1, n_f):
-            src = lax.rem(z + s, n_f)
-            for d in range(1, n_g):
-                owner = lax.rem(grp + d, n_g)
-                ref = pieces[p][1](src, owner)
-                pltpu.make_async_remote_copy(
-                    src_ref=ref, dst_ref=ref, send_sem=ys.at[p, src * n_g],
-                    recv_sem=yr.at[p, src * n_g + owner],
-                    device_id=(owner, z, t), device_id_type=MESH).wait_recv()
+            arrive_from(p, lax.rem(z + s, n_f))
 
     state = {"own": 0, "ev": 0}
-    order = [(p, s) for p in range(n_p) for s in range(1, n_f)]
+    downs = [i for i, pc in enumerate(pieces) if pc[0] == "down"]
+    by_source = per_block == 1
+    order = [(p, s) for p in range(n_p) for s in range(1, n_f) if not (by_source and p in downs)]
+    if by_source:
+        order += [(p, s) for s in range(1, n_f) for p in downs]
 
     def send_own(upto):
         while state["own"] < min(upto, n_p):
@@ -154,7 +162,7 @@
         for _ in range(count):
             if state["ev"] < len(order):
                 p, s = order[state["ev"]]
-                send_own(p + 2)
+                send_own(p + 3)
                 event(p, s)
                 state["ev"] += 1
 
@@ -224,7 +232,7 @@
             src_ref=src_ref, dst_ref=dst_ref, send_sem=ssem, recv_sem=rsem,
             device_id=(grp, z, dest), device_id_type=MESH)
 
-    def reduce(lhs, rhs, prt, r_a, stage, r_b, sems, base, emit, between):
+    def reduce(lhs, rhs, prt, r_a, stage, r_b, sems, base, emit):
         s1, r1, s2, r2 = sems
 
         def to_partner(d, r):
@@ -253,8 +261,10 @@
             if prev is not None and prev[0] > 0:
                 combine(*prev)
             prev = (d, r)
-            between()
+            if r % 2 == 1:
+                pump(1)
         for r in range(R):
+            pump(1)
             to_partner(0, r).wait_recv()
             total = prt[t, rows_of(r), :].astype(F32) + r_a[0, rows_of(r), :].astype(F32)
             for d in range(1, n_x):
@@ -295,8 +305,9 @@
                     part_h * cos_ref[rows, :] + pltpu.roll(part_h, HEAD // 2, 1) * sin_ref[rows, :]).astype(BF)
         return 0
 
-    lax.fori_loop(0, R, project, 0)
-    pump(2)
+    for r in range(R):
+        project(r, 0)
+        pump(1)
     for h in range(heads):
         cols = slice(h * HEAD, (h + 1) * HEAD)
         for r in range(R):
@@ -314,22 +325,24 @@
             kept = kept * lax.rsqrt(jnp.mean(kept * kept, axis=-1, keepdims=True) + EPS)
             gate = gr[r * RC:(r + 1) * RC, cols].astype(F32)
             ho[r * RC:(r + 1) * RC, cols] = (kept * hg[:, cols] * (gate / (1.0 + jnp.exp(-gate)))).astype(BF)
+            if r != 1:
+                pump(1)
     arrive_all("out")
-    send_own(6)
     agm = (c1s, c1r, c2s, c2r)
 
     def emit_mixed(r, val):
         mw[t, rows_of(r), :] = val
         ag_start(mw, r, agm)
 
-    reduce(ho, ob, part, ra, st, rb, (b1s, b1r, b2s, b2r), xw, emit_mixed, lambda: None)
-    pump(1)
+    reduce(ho, ob, part, ra, st, rb, (b1s, b1r, b2s, b2r), xw, emit_mixed)
     for r in range(R):
         ag_forward(mw, r, agm)
-    pump(1)
+        if r % 2 == 0:
+            pump(1)
     for r in range(R):
         ag_finish(mw, r, agm)
         norm_rows(mw, cg, r)
+        pump(1)
     arrive_all("up")
 
     lift[0:16, :] = jnp.zeros((16, F), BF)
@@ -359,14 +372,76 @@
 
     for r in range(R):
         widen(sb, swit, r)
-        lax.fori_loop(r * (RC // 64), (r + 1) * (RC // 64), conv_rows, 0)
         pump(1)
-    arrive_all("down")
+        for part_r in range(2):
+            first = r * (RC // 64) + part_r * (RC // 128)
+            lax.fori_loop(first, first + RC // 128, conv_rows, 0)
+            pump(1)
 
     def emit_out(r, val):
         o_ref[rows_of(r), :] = val
 
-    reduce(hid, db, part2, ra2, st2, rb2, (d1s, d1r, d2s, d2r), mw, emit_out, lambda: None)
+    def slot_reduce(s, way):
+        slot = z - s if way == 0 else z + s
+        here = (slot >= 0) if way == 0 else (slot < n_f)
+        b = jnp.clip(slot, 0, n_f - 1)
+        bx, bc = b // 2, b % 2
+        d = lax.rem(bx - x + n_x, n_x)
+        to_other = jnp.logical_and(here, bc != c)
+        relay = jnp.logical_and(jnp.logical_and(here, bc == c), bx != x)
+        if s > 0:
+            @pl.when(here)
+            def _():
+                for p in downs:
+                    arrive_from(p, b)
+        ups, outs = [], []
+        for r in range(R):
+            up = rs2(part2.at[b, rows_of(r), :], ra2.at[d, rows_of(r), :], partner, d1s.at[d, r], d1r.at[d, r])
+            out = rs2(st2.at[d, rows_of(r), :], rb2.at[d, rows_of(r), :], bx * 2 + c, d2s.at[d, r], d2r.at[d, r])
+            pending.append((to_other, up))
+            pending.append((relay, out))
+            ups.append(up)
+            outs.append(out)
+
+        for r in range(R):
+            @pl.when(here)
+            def _(r=r):
+                product(hid, db, part2, b, r)
+
+            @pl.when(to_other)
+            def _(r=r):
+                ups[r].start()
+
+        def second():
+            for r in range(R):
+                @pl.when(relay)
+                def _(r=r):
+                    ups[r].wait_recv()
+                    st2[d, rows_of(r), :] = (part2[b, rows_of(r), :].astype(F32)
+                                             + ra2[d, rows_of(r), :].astype(F32)).astype(BF)
+                    outs[r].start()
+        return second
+
+    rs2 = rs_copy
+    if by_source:
+        slot_reduce(0, 0)()
+        for s in range(1, n_f):
+            while state["ev"] < len(order) and order[state["ev"]][1] <= s:
+                pump()
+            later = [slot_reduce(s, way) for way in (0, 1)]
+            for act in later:
+                act()
+        for r in range(R):
+            rs2(part2.at[t, rows_of(r), :], ra2.at[0, rows_of(r), :], partner, d1s.at[0, r], d1r.at[0, r]).wait_recv()
+            total = part2[t, rows_of(r), :].astype(F32) + ra2[0, rows_of(r), :].astype(F32)
+            for d in range(1, n_x):
+                rs2(st2.at[d, rows_of(r), :], rb2.at[d, rows_of(r), :], lax.rem(x + d, n_x) * 2 + c,
+                    d2s.at[d, r], d2r.at[d, r]).wait_recv()
+                total = total + rb2[d, rows_of(r), :].astype(F32)
+            emit_out(r, (mw[t, rows_of(r), :].astype(F32) + total).astype(BF))
+    else:
+        arrive_all("down")
+        reduce(hid, db, part2, ra2, st2, rb2, (d1s, d1r, d2s, d2r), mw, emit_out)
 
     for cond, cp in pending:
         if cond is None:
@@ -396,7 +471,7 @@
     ids = (lax.axis_index("tp") * heads + jnp.arange(heads, dtype=jnp.int32)).astype(F32)
     rate = jnp.broadcast_to(jnp.log1p(-jnp.exp2(-5.0 - ids))[:, None], (heads, 128))
 
-    n_p = (chunks_of(fr // n_g) * 3 + 1 + chunks_of(down_weight.shape[0] // n_g))
+    n_p = (chunks_of(fr // n_g) * 3 + 1 + chunks_of(down_weight.shape[0] // n_g, 4))
     R = T // 256
     dma = pltpu.SemaphoreType.DMA
     anyspec = pl.BlockSpec(memory_space=pl.ANY)

time: 286 us -> 236 us (0.83)
  Pallas kernels: 278 us -> 230 us
    pallas_call x1, Pallas kernels: 278 us -> 230 us  [on_device(): call(inputs, mixer_gain[None, :], query_weight, key_weight, value_weight,...]
where the time goes in v2:
time: 236 us
  Pallas kernels  230 us (97%)
  local copies, waits for them, and re-layouts  2.68 us (1%)
  other arithmetic  2.62 us (1%)
    pallas_call x1, Pallas kernels, on_device(): call(inputs, mixer_gain[None, :], query_weight, key_weight, value_weight,...  230 us

profile of v2, /device:TPU:3, one launch (start us, length us, event | category | flops | bytes accessed | tf_op | source)
XLA Modules:
  0.0 235.7 jit_solution(2523855198774405907)
XLA Ops:
  0.0 1.5 fusion
  1.5 1.1 pad_maximum_fusion
  2.6 0.6 broadcast_in_dim.20.ld_ref
  3.2 230.4 %shard_map.136 = bf16[768,512]{1,0:T(8,128)(2,1)} custom-call(bf16[768,512]{1,0:T(8,128)(2,1)} %x_hbm.1, f32[1,2048]{1,0:T(1,128)} %bitcast.3, bf16[512,256]{1,0:T(8,128)(2,1)} %q_hbm.1, bf16[512,256]{1,0:T(8,128)(2,1)} %k_hbm.1, bf16[512,256]{1,0:T(8,128)(2,1)} %v_hbm.1, bf16[512,256]{1,0:T(8,128)(2,1)} %g_hbm.1, f32[1,256]{1,0:T(1,128)} %bitcast.5, ...), custom_call_target="tpu_custom_call" | custom-call | flops 17314086912 | bytes 17301504 | tf_op jit(solution)/shard_map/pallas_call | solution.py:512
  233.6 2.1 copy.16
  (3 shorter events, 0.0 us)
